TPU v7x, 32 devices: a whole 2x2x4 slice. The times are simulated.
32 devices in a mesh: ep: 8 (over z, x), tp: 4 (over y, core).
Axes of the slice: x: 2, y: 2, z: 4, core: 2. Of those that a mesh axis runs over, the one named last changes fastest.
Arguments:
- conv_value: bfloat16 [4096, 2048], P('ep', 'tp'), may hold values from -6 to 6
- conv_gate: bfloat16 [4096, 2048], P('ep', 'tp'), may hold values from -9 to 9
- conv_taps: float32 [31, 2048], P(None, 'tp'), may hold values from -14 to 14
- norm_gain: float32 [2048], P('tp'), may hold values from 0.1 to 1.9
- norm_shift: float32 [2048], P('tp'), may hold values from -3 to 3
- conv_out_weight: bfloat16 [2048, 2048], P(None, 'tp'), may hold values from -0.125 to 0.125
- moe_input: bfloat16 [1024, 2048], P('ep'), may hold values from -6 to 6
- moe_gain: float32 [2048], replicated, may hold values from 0.1 to 1.9
- routes: int32 [1024, 4], P('ep'), may hold values from 0 to 7, all different within a row; in each aligned block of 128 rows (0 to 127, 128 to 255, ...) at most 128 rows name the same one
- route_weights: float32 [1024, 4], P('ep'), may hold values from 0.25 to 1
- expert_gate: bfloat16 [8, 2048, 4096], P('ep', None, 'tp'), may hold values from -0.125 to 0.125
- expert_up: bfloat16 [8, 2048, 4096], P('ep', None, 'tp'), may hold values from -0.125 to 0.125
- expert_down: bfloat16 [8, 4096, 2048], P('ep', None, 'tp'), may hold values from -0.09375 to 0.09375
- shared_gate: bfloat16 [2048, 512], P(None, 'tp'), may hold values from -0.125 to 0.125
- shared_up: bfloat16 [2048, 512], P(None, 'tp'), may hold values from -0.125 to 0.125
- shared_down: bfloat16 [512, 2048], P(None, 'tp'), may hold values from -0.25 to 0.25
Outputs:
- conv_result: bfloat16 [4096, 2048], P('ep', 'tp')
- moe_result: bfloat16 [1024, 2048], P('ep', 'tp')
Inputs may be any that keep to these rules, and one draw needn't show every extreme that they name: `routes`: in the rows of one device (aligned blocks of 128 rows) no expert is named by more than 128 rows, a bound that some block reaches; each row names 4 different experts.
All inputs are finite; a program needn't handle non-finite values.
Results may differ from a plain program's by a relative error of at most 0.0068.
Values may be sent and summed in bfloat16 or wider, within the bound.
A program may use at most 64 MiB of HBM per device.

v0:
```python
import jax
import jax.numpy as jnp
from jax import lax
from jax.sharding import PartitionSpec as P


def from_behind(value, axis, steps):
    count = lax.axis_size(axis)
    initial, last = (max(0, -steps), min(count, count - steps))
    return lax.ppermute(value, axis, [(source, source + steps) for source in range(initial, last)])


def body(
    conv_value,
    conv_gate,
    conv_taps,
    norm_gain,
    norm_shift,
    conv_out_weight,
    moe_input,
    moe_gain,
    routes,
    route_weights,
    expert_gate,
    expert_up,
    expert_down,
    shared_gate,
    shared_up,
    shared_down,
):
    tap_count = conv_taps.shape[0]
    rows_a = conv_value.shape[0]
    glu_rows = (
        conv_value.astype(jnp.float32) * jax.nn.sigmoid(conv_gate.astype(jnp.float32))
    ).astype(jnp.bfloat16)
    before = from_behind(glu_rows[rows_a - (tap_count - 1) :], "ep", 1)
    padded = jnp.concatenate([before, glu_rows], axis=0)
    filtered = jnp.zeros(glu_rows.shape, jnp.float32)
    for offset in range(tap_count):
        filtered = filtered + conv_taps[offset] * padded[offset : offset + rows_a].astype(
            jnp.float32
        )
    row_total, squares = lax.psum(
        (jnp.sum(filtered, axis=1), jnp.sum(filtered * filtered, axis=1)), "tp"
    )
    channels = conv_out_weight.shape[0]
    row_mean = row_total / channels
    row_square = squares / channels
    scaled = (filtered - row_mean[:, None]) * lax.rsqrt(row_square - row_mean * row_mean + 1e-05)[
        :, None
    ]
    conv_hidden = jax.nn.silu(scaled * norm_gain + norm_shift).astype(jnp.bfloat16)
    conv_sum = jnp.dot(
        lax.all_gather(conv_hidden, "tp", axis=1, tiled=True),
        conv_out_weight,
        preferred_element_type=jnp.float32,
    )
    conv_result = conv_sum.astype(jnp.bfloat16)
    inputs = moe_input.astype(jnp.float32)
    normed = (
        inputs * lax.rsqrt(jnp.mean(inputs * inputs, axis=1, keepdims=True) + 1e-06) * moe_gain
    ).astype(jnp.bfloat16)
    rows_b, per_row = routes.shape
    model_width = normed.shape[1]
    groups = lax.axis_size("ep")
    capacity = 2 * rows_b * per_row // groups
    flat_expert = routes.reshape(-1)
    owner_row = jnp.arange(rows_b * per_row, dtype=jnp.int32) // per_row
    expert_hits = (flat_expert[:, None] == jnp.arange(groups, dtype=jnp.int32)[None, :]).astype(
        jnp.int32
    )
    slot_rank = jnp.sum((jnp.cumsum(expert_hits, axis=0) - expert_hits) * expert_hits, axis=1)
    slot_index = flat_expert * capacity + slot_rank
    outgoing = (
        jnp.zeros((groups * capacity, model_width), jnp.bfloat16)
        .at[slot_index]
        .set(normed[owner_row])
    )
    outgoing = outgoing.reshape(groups, capacity, model_width)
    slot_share = capacity // lax.axis_size("tp")
    own_slots = lax.dynamic_slice_in_dim(outgoing, lax.axis_index("tp") * slot_share, slot_share, 1)
    partial_rows = lax.all_to_all(own_slots, "ep", split_axis=0, concat_axis=0, tiled=True)
    arrived = lax.all_gather(partial_rows, "tp", axis=1, tiled=True)
    arrived_rows = arrived.reshape(groups * capacity, model_width)
    gate_value = jnp.dot(arrived_rows, expert_gate[0], preferred_element_type=jnp.float32)
    upward = jnp.dot(arrived_rows, expert_up[0], preferred_element_type=jnp.float32)
    expert_hidden = (jax.nn.silu(gate_value) * upward).astype(jnp.bfloat16)
    shared_hidden = (
        jax.nn.silu(jnp.dot(normed, shared_gate, preferred_element_type=jnp.float32))
        * jnp.dot(normed, shared_up, preferred_element_type=jnp.float32)
    ).astype(jnp.bfloat16)
    columns = expert_down.shape[2]
    routed_rows = expert_down[0]
    routed_sum = jnp.dot(
        lax.all_gather(expert_hidden, "tp", axis=1, tiled=True),
        routed_rows,
        preferred_element_type=jnp.float32,
    )
    shared_sum = jnp.dot(
        lax.all_gather(shared_hidden, "tp", axis=1, tiled=True),
        shared_down,
        preferred_element_type=jnp.float32,
    )
    expert_out = routed_sum.astype(jnp.bfloat16).reshape(groups, capacity, columns)
    returned = lax.all_to_all(expert_out, "ep", split_axis=0, concat_axis=0, tiled=True).reshape(
        groups * capacity, columns
    )
    picked = returned[slot_index].astype(jnp.float32) * route_weights.reshape(-1)[:, None]
    moe_sum = jnp.sum(picked.reshape(rows_b, per_row, columns), axis=1) + shared_sum
    return (conv_result, moe_sum.astype(jnp.bfloat16))


def solution(mesh):
    return jax.shard_map(
        body,
        mesh=mesh,
        in_specs=(
            P("ep", "tp"),
            P("ep", "tp"),
            P(None, "tp"),
            P("tp"),
            P("tp"),
            P(None, "tp"),
            P("ep", None),
            P(),
            P("ep", None),
            P("ep", None),
            P("ep", None, "tp"),
            P("ep", None, "tp"),
            P("ep", None, "tp"),
            P(None, "tp"),
            P(None, "tp"),
            P(None, "tp"),
        ),
        out_specs=(P("ep", "tp"), P("ep", "tp")),
        check_vma=False,
    )
```

profile of v0, /device:TPU:0, one launch (start us, length us, event | category | flops | bytes accessed | tf_op | source)
XLA Modules:
  0.0 221.6 jit_solution(14922758619860375159)
XLA Ops:
  9.1 1.2 fusion.16
  12.1 1.2 fusion.18
  13.3 12.8 %scatter_custom_fusion = bf16[1024,2048]{1,0:T(8,128)(2,1)} fusion(s32[512]{0:T(512)S(1)} %bitcast.105, bf16[128,2048]{1,0:T(8,128)(2,1)S(1)} %fusion.18, s32[1024]{0:T(1024)S(1)} %pad_clamp_fusion.1, bf16[]{:T(256)} %constant.46.clone.1), kind=kCustom, calls=%fused_computation.39 | custom fusion | bytes 4194306 | tf_op jit(solution)/shard_map/scatter | solution.py:77
  26.1 1.3 constant_dynamic-slice_fusion
  27.4 32.9 %all_to_all.10 = bf16[8,32,2048]{2,1,0:T(8,128)(2,1)} all-to-all(bf16[8,32,2048]{2,1,0:T(8,128)(2,1)S(1)} %constant_dynamic-slice_fusion), channel_id=1, replica_groups=mesh['ep'=8,'tp'=4] {'ep'}, dimensions={0} | all-to-all | bytes 2097152 | tf_op jit(solution)/shard_map/all_to_all | solution.py:82
  60.4 33.6 %all-gather.6.cloned.1.call-done = bf16[8,128,2048]{2,1,0:T(8,128)(2,1)} async-done(((bf16[8,32,2048]{2,1,0:T(8,128)(2,1)}), bf16[8,128,2048]{2,1,0:T(8,128)(2,1)}) %all-gather.6.cloned.1.call-update) | async-done | bytes 4194320 | tf_op jit(solution)/shard_map/all_gather | solution.py:83
  94.0 7.6 %fusion.2 = f32[1024,1024]{1,0:T(8,128)S(1)} fusion(bf16[1024,2048]{1,0:T(8,128)(2,1)} %bitcast.109, bf16[1,2048,1024]{2,1,0:T(8,128)(2,1)} %param.27), kind=kOutput, calls=%fused_computation.34 | convolution fusion | flops 4294967296 | bytes 12582912 | tf_op jit(solution)/shard_map/dot_general | solution.py:86
  101.8 6.3 %multiply_convert_fusion = bf16[1024,1024]{1,0:T(8,128)(2,1)} fusion(f32[1024,1024]{1,0:T(8,128)S(1)} %fusion.2, bf16[1024,2048]{1,0:T(8,128)(2,1)S(1)} %bitcast.110, bf16[1,2048,1024]{2,1,0:T(8,128)(2,1)S(1)} %copy-done.8), kind=kOutput, calls=%fused_computation.38 | convolution fusion | flops 4301258752 | bytes 14680064 | tf_op jit(solution)/shard_map/dot_general | solution.py:85
  108.5 3.4 %collective-permute-start = (bf16[30,512]{1,0:T(8,128)(2,1)S(1)}, bf16[30,512]{1,0:T(8,128)(2,1)S(1)}, u32[]{:S(2)}, u32[]{:S(2)}) collective-permute-start(bf16[30,512]{1,0:T(8,128)(2,1)S(1)} %slice.260), channel_id=1, source_target_pairs={{0,4},{4,8},{8,12},{12,16},{16,20},{20,24},{24,28},{1,5},{5,9},{9,... | collective-permute-start | bytes 92168 | tf_op jit(solution)/shard_map/ppermute | solution.py:10
  112.0 1.5 collective-permute-done
  113.5 4.8 %fusion.51 = (f32[512]{0:T(512)S(1)}, f32[512]{0:T(512)S(1)}, f32[512,512]{1,0:T(8,128)S(1)}) fusion(bf16[512,512]{1,0:T(8,128)(2,1)S(1)} %multiply_convert_fusion.2, f32[512]{0:T(512)S(1)} %bitcast.103, bf16[30,512]{1,0:T(8,128)(2,1)S(1)} %collective-permute-done, f32[512]{0:T(512)S(1)} %bitcast.104, f32[512]{0:T(512)S(1)} %bitcast.75, ...), kind=kLoop, calls=%fused_computation.113 | loop fusion | flops 48495616 | bytes 1671168 | tf_op jit(solution)/shard_map/reduce_sum | solution.py:44
  118.3 6.5 %all-reduce = (f32[512]{0:T(512)S(1)}, f32[512]{0:T(512)S(1)}) all-reduce(f32[512]{0:T(512)S(1)} %get-tuple-element.3, f32[512]{0:T(512)S(1)} %get-tuple-element.2), channel_id=1, replica_groups=mesh['ep'=8,'tp'=4] {'tp'}, use_global_device_ids=true, to_apply=%region_3.0 | all-reduce | flops 1024 | bytes 8192 | tf_op jit(solution)/shard_map/psum | solution.py:43
  124.8 1.2 multiply_convert_fusion.1
  126.1 40.6 %all-gather.8.cloned.1.call-done = bf16[1024,4096]{1,0:T(8,128)(2,1)} async-done(((bf16[1024,1024]{1,0:T(8,128)(2,1)}), bf16[1024,4096]{1,0:T(8,128)(2,1)}) %all-gather.8.cloned.1.call-update) | async-done | bytes 8388624 | tf_op jit(solution)/shard_map/all_gather | solution.py:95
  166.7 10.0 %fusion.11 = bf16[1024,512]{1,0:T(8,128)(2,1)} fusion(bf16[1024,4096]{1,0:T(8,128)(2,1)} %all-gather.8.cloned.1.call-done, bf16[1,4096,512]{2,1,0:T(8,128)(2,1)} %param.28), kind=kOutput, calls=%fused_computation.42 | convolution fusion | flops 4295491584 | bytes 13631488 | tf_op jit(solution)/shard_map/dot_general | solution.py:94
  176.7 5.5 %all-to-all-start.1 = ((bf16[8,128,512]{2,1,0:T(8,128)(2,1)}), bf16[8,128,512]{2,1,0:T(8,128)(2,1)S(1)}, u32[]{:S(2)}, u32[]{:S(2)}) async-start(bf16[8,128,512]{2,1,0:T(8,128)(2,1)} %bitcast.73), calls=%async_computation.1 | async-start | bytes 2097152 | tf_op jit(solution)/shard_map/all_to_all | solution.py:105
  182.3 1.5 fusion.54
  183.8 1.5 fusion.15
  185.3 6.1 %all_gather.15 = bf16[128,512]{1,0:T(8,128)(2,1)S(1)} all-gather(bf16[128,128]{1,0:T(8,128)(2,1)S(1)} %fusion.15), channel_id=1, replica_groups=mesh['ep'=8,'tp'=4] {'tp'}, dimensions={1}, use_global_device_ids=true | all-gather | bytes 163840 | tf_op jit(solution)/shard_map/all_gather | solution.py:100
  192.1 3.6 %convolution_convert_fusion = bf16[512,512]{1,0:T(8,128)(2,1)} fusion(bf16[512,2048]{1,0:T(8,128)(2,1)} %all-gather.4.cloned.1.call-done, bf16[2048,512]{1,0:T(8,128)(2,1)S(1)} %copy-done), kind=kOutput, calls=%fused_computation.45 | convolution fusion | flops 1074003968 | bytes 4718592 | tf_op jit(solution)/shard_map/dot_general | solution.py:53
  195.7 12.7 %all-to-all-done.1 = bf16[8,128,512]{2,1,0:T(8,128)(2,1)S(1)} async-done(((bf16[8,128,512]{2,1,0:T(8,128)(2,1)}), bf16[8,128,512]{2,1,0:T(8,128)(2,1)S(1)}, u32[]{:S(2)}, u32[]{:S(2)}) %all-to-all-start.1) | async-done | bytes 1048608 | tf_op jit(solution)/shard_map/all_to_all | solution.py:105
  208.4 2.6 %gather_fusion = bf16[512,512]{1,0:T(8,128)(2,1)} fusion(bf16[1024,512]{1,0:T(8,128)(2,1)S(1)} %bitcast.71, s32[1024]{0:T(1024)S(1)} %pad_clamp_fusion), kind=kCustom, calls=%fused_computation.1 | custom fusion | bytes 1050624 | tf_op jit(solution)/shard_map/gather | solution.py:108
  211.0 1.4 reshape.133
  213.1 1.9 fusion.14
  (51 shorter events, 5.7 us)
Async XLA Ops:
  7.2 184.9 %copy-start = (bf16[2048,512]{1,0:T(8,128)(2,1)S(1)}, bf16[2048,512]{1,0:T(8,128)(2,1)}, u32[]{:S(2)}) copy-start(bf16[2048,512]{1,0:T(8,128)(2,1)} %param.21) | copy-start | bytes 6291460
  7.2 86.9 %all-gather.6.cloned.1.call-start = ((), (), s32[]{:S(2)}) async-start(), calls=%async_computation.3 | async-start | bytes 5242880 | tf_op jit(solution)/shard_map/all_gather | solution.py:83
  13.3 47.1 %copy-start.1 = (bf16[128,2048]{1,0:T(8,128)(2,1)}, bf16[128,2048]{1,0:T(8,128)(2,1)S(1)}, u32[]{:S(2)}) copy-start(bf16[128,2048]{1,0:T(8,128)(2,1)S(1)} %fusion.18) | copy-start | bytes 1572868
  60.4 106.3 %all-gather.8.cloned.1.call-start = ((), (), s32[]{:S(2)}) async-start(), calls=%async_computation.4 | async-start | bytes 10485760 | tf_op jit(solution)/shard_map/all_gather | solution.py:95
  94.0 7.7 %copy-start.8 = (bf16[1,2048,1024]{2,1,0:T(8,128)(2,1)S(1)}, bf16[1,2048,1024]{2,1,0:T(8,128)(2,1)}, u32[]{:S(2)}) copy-start(bf16[1,2048,1024]{2,1,0:T(8,128)(2,1)} %param.26) | copy-start | bytes 12582916
  94.0 7.7 %copy-start.9 = (bf16[8,128,2048]{2,1,0:T(8,128)(2,1)S(1)}, bf16[8,128,2048]{2,1,0:T(8,128)(2,1)}, u32[]{:S(2)}) copy-start(bf16[8,128,2048]{2,1,0:T(8,128)(2,1)} %all-gather.6.cloned.1.call-done) | copy-start | bytes 12582916
  101.7 6.4 %copy-start.2 = (bf16[512,512]{1,0:T(8,128)(2,1)S(1)}, bf16[512,512]{1,0:T(8,128)(2,1)}, u32[]{:S(2)}) copy-start(bf16[512,512]{1,0:T(8,128)(2,1)} %param.17) | copy-start | bytes 1572868
  101.7 6.4 %copy-start.3 = (bf16[512,512]{1,0:T(8,128)(2,1)S(1)}, bf16[512,512]{1,0:T(8,128)(2,1)}, u32[]{:S(2)}) copy-start(bf16[512,512]{1,0:T(8,128)(2,1)} %param.16) | copy-start | bytes 1572868
  101.7 10.1 %copy-start.4 = (f32[31,512]{1,0:T(8,128)S(1)}, f32[31,512]{1,0:T(8,128)}, u32[]{:S(2)}) copy-start(f32[31,512]{1,0:T(8,128)} %param.18) | copy-start | bytes 190468
  108.1 16.7 %copy-start.5 = (f32[512]{0:T(512)S(1)}, f32[512]{0:T(512)}, u32[]{:S(2)}) copy-start(f32[512]{0:T(512)} %param.20) | copy-start | bytes 6148
  108.1 16.7 %copy-start.6 = (f32[512]{0:T(512)S(1)}, f32[512]{0:T(512)}, u32[]{:S(2)}) copy-start(f32[512]{0:T(512)} %param.19) | copy-start | bytes 6148
  108.1 84.0 %all-gather.4.cloned.1.call-start = ((), (), s32[]{:S(2)}) async-start(), calls=%async_computation.2 | async-start | bytes 2621440 | tf_op jit(solution)/shard_map/all_gather | solution.py:54
  108.5 5.0 %collective-permute-start = (bf16[30,512]{1,0:T(8,128)(2,1)S(1)}, bf16[30,512]{1,0:T(8,128)(2,1)S(1)}, u32[]{:S(2)}, u32[]{:S(2)}) collective-permute-start(bf16[30,512]{1,0:T(8,128)(2,1)S(1)} %slice.260), channel_id=1, source_target_pairs={{0,4},{4,8},{8,12},{12,16},{16,20},{20,24},{24,28},{1,5},{5,9},{9,... | collective-permute-start | bytes 92168 | tf_op jit(solution)/shard_map/ppermute | solution.py:10
  126.1 56.1 %copy-start.7 = (f32[128,4]{0,1:T(4,128)S(1)}, f32[128,4]{0,1:T(4,128)}, u32[]{:S(2)}) copy-start(f32[128,4]{0,1:T(4,128)} %param.25) | copy-start | bytes 6148
  176.7 31.7 %all-to-all-start.1 = ((bf16[8,128,512]{2,1,0:T(8,128)(2,1)}), bf16[8,128,512]{2,1,0:T(8,128)(2,1)S(1)}, u32[]{:S(2)}, u32[]{:S(2)}) async-start(bf16[8,128,512]{2,1,0:T(8,128)(2,1)} %bitcast.73), calls=%async_computation.1 | async-start | bytes 2097152 | tf_op jit(solution)/shard_map/all_to_all | solution.py:105
Sparse Core Ops, SparseCore 0:
  60.5 33.4 all-gather.5
  108.2 58.3 all-gather.7
  168.8 23.2 all-gather.3
where the time goes:
time: 222 us
  waiting for transfers between devices  89.1 us (40%)
  blocking collectives  45.5 us (20%)
  matrix products  32.5 us (15%)
  local copies, waits for them, and re-layouts  19.8 us (9%)
  between operations  14 us (6%)
  other arithmetic  11.7 us (5%)
  starting transfers between devices  9.02 us (4%)
    all_gather x1, waiting for transfers between devices, body(): lax.all_gather(expert_hidden, 'tp', axis=1, tiled=True)  40.6 us
    all_gather x1, waiting for transfers between devices, body(): arrived = lax.all_gather(partial_rows, 'tp', axis=1, tiled=True)  33.6 us
    all_to_all x1, blocking collectives, body(): lax.all_to_all(own_slots, 'ep', split_axis=0, concat_axis=0, tiled=True)  32.9 us
    scatter x1, local copies, waits for them, and re-layouts, body(): outgoing = jnp.zeros((groups * capacity, model_width), jnp.bfloat16).at[s...  12.8 us
    all_to_all x1, waiting for transfers between devices, body(): lax.all_to_all(expert_out, 'ep', split_axis=0, concat_axis=0, tiled=True)  12.7 us
    dot_general x1, matrix products, body(): jnp.dot(lax.all_gather(expert_hidden, 'tp', axis=1, tiled=True), routed_r...  10 us
    dot_general x1, matrix products, body(): jnp.dot(arrived_rows, expert_up[0], preferred_element_type=jnp.float32)  7.64 us
    psum x1, blocking collectives, body(): lax.psum((jnp.sum(filtered, axis=1), jnp.sum(filtered * filtered, axis=1)...  6.48 us
  transfers between devices with their start and end apart: 5, of which 5 were waited for; matrix products, arithmetic and copies ran while one was open for 10% of the time, Pallas kernels for 0%

commit v1 on v0

--- a/solution.py
+++ b/solution.py
@@ -2,6 +2,11 @@
 import jax.numpy as jnp
 from jax import lax
 from jax.sharding import PartitionSpec as P
+
+
+def treat_yards_all(message, lane_axis):
+    then = jnp.concatenate(lax.all_gather(message, lane_axis), axis=1)
+    return then
 
 
 def from_behind(value, axis, steps):
@@ -92,9 +97,7 @@
     columns = expert_down.shape[2]
     routed_rows = expert_down[0]
     routed_sum = jnp.dot(
-        lax.all_gather(expert_hidden, "tp", axis=1, tiled=True),
-        routed_rows,
-        preferred_element_type=jnp.float32,
+        treat_yards_all(expert_hidden, "tp"), routed_rows, preferred_element_type=jnp.float32
     )
     shared_sum = jnp.dot(
         lax.all_gather(shared_hidden, "tp", axis=1, tiled=True),

time: 222 us -> 234 us (1.054)
  local copies, waits for them, and re-layouts: 19.8 us -> 31.2 us
    all_gather x0 -> x1, local copies, waits for them, and re-layouts: none -> 11.5 us  [treat_yards_all(): then = jnp.concatenate(lax.all_gather(message, lane_axis), axis=1)]
  transfers between devices with their start and end apart: 5 -> 5, of which waited for: 5 -> 4; matrix products, arithmetic and copies ran while one was open for 10% -> 15% of each run, Pallas kernels for 0% -> 0%
where the time goes in v1:
time: 234 us; the launch traced here: 233 us
  waiting for transfers between devices  89.6 us (38%)
  blocking collectives  45.1 us (19%)
  matrix products  32.7 us (14%)
  local copies, waits for them, and re-layouts  31.2 us (13%)
  between operations  14 us (6%)
  other arithmetic  11.7 us (5%)
  starting transfers between devices  9.01 us (4%)
    all_gather x1, waiting for transfers between devices, treat_yards_all(): then = jnp.concatenate(lax.all_gather(message, lane_axis), axis=1)  40.6 us
    all_gather x1, waiting for transfers between devices, body(): arrived = lax.all_gather(partial_rows, 'tp', axis=1, tiled=True)  33.6 us
    all_to_all x1, blocking collectives, body(): lax.all_to_all(own_slots, 'ep', split_axis=0, concat_axis=0, tiled=True)  32.9 us
    all_to_all x1, waiting for transfers between devices, body(): lax.all_to_all(expert_out, 'ep', split_axis=0, concat_axis=0, tiled=True)  13.8 us
    scatter x1, local copies, waits for them, and re-layouts, body(): outgoing = jnp.zeros((groups * capacity, model_width), jnp.bfloat16).at[s...  12.8 us
    all_gather x1, local copies, waits for them, and re-layouts, treat_yards_all(): then = jnp.concatenate(lax.all_gather(message, lane_axis), axis=1)  11.5 us
    dot_general x1, matrix products, body(): jnp.dot(treat_yards_all(expert_hidden, 'tp'), routed_rows, preferred_elem...  10.1 us
    dot_general x1, matrix products, body(): jnp.dot(arrived_rows, expert_up[0], preferred_element_type=jnp.float32)  7.64 us
  transfers between devices with their start and end apart: 5, of which 4 were waited for; matrix products, arithmetic and copies ran while one was open for 15% of the time, Pallas kernels for 0%

profile of v1, /device:TPU:0, one launch (start us, length us, event | category | flops | bytes accessed | tf_op | source)
XLA Modules:
  0.0 233.2 jit_solution(5762401831842666973)
XLA Ops:
  9.1 1.2 fusion.16
  12.1 1.2 fusion.18
  13.3 12.8 %scatter_custom_fusion = bf16[1024,2048]{1,0:T(8,128)(2,1)} fusion(s32[512]{0:T(512)S(1)} %bitcast.111, bf16[128,2048]{1,0:T(8,128)(2,1)S(1)} %fusion.18, s32[1024]{0:T(1024)S(1)} %pad_clamp_fusion.1, bf16[]{:T(256)} %constant.46.clone.1), kind=kCustom, calls=%fused_computation.39 | custom fusion | bytes 4194306 | tf_op jit(solution)/shard_map/scatter | solution.py:82
  26.1 1.3 constant_dynamic-slice_fusion
  27.4 32.9 %all_to_all.10 = bf16[8,32,2048]{2,1,0:T(8,128)(2,1)} all-to-all(bf16[8,32,2048]{2,1,0:T(8,128)(2,1)S(1)} %constant_dynamic-slice_fusion), channel_id=1, replica_groups=mesh['ep'=8,'tp'=4] {'ep'}, dimensions={0} | all-to-all | bytes 2097152 | tf_op jit(solution)/shard_map/all_to_all | solution.py:87
  60.4 33.6 %all-gather.7.cloned.1.call-done = bf16[8,128,2048]{2,1,0:T(8,128)(2,1)} async-done(((bf16[8,32,2048]{2,1,0:T(8,128)(2,1)}), bf16[8,128,2048]{2,1,0:T(8,128)(2,1)}) %all-gather.7.cloned.1.call-update) | async-done | bytes 4194320 | tf_op jit(solution)/shard_map/all_gather | solution.py:88
  94.0 7.6 %fusion.2 = f32[1024,1024]{1,0:T(8,128)S(1)} fusion(bf16[1024,2048]{1,0:T(8,128)(2,1)} %bitcast.115, bf16[1,2048,1024]{2,1,0:T(8,128)(2,1)} %param.27), kind=kOutput, calls=%fused_computation.34 | convolution fusion | flops 4294967296 | bytes 12582912 | tf_op jit(solution)/shard_map/dot_general | solution.py:91
  101.8 6.4 %multiply_convert_fusion = bf16[1024,1024]{1,0:T(8,128)(2,1)} fusion(f32[1024,1024]{1,0:T(8,128)S(1)} %fusion.2, bf16[1024,2048]{1,0:T(8,128)(2,1)S(1)} %bitcast.116, bf16[1,2048,1024]{2,1,0:T(8,128)(2,1)S(1)} %copy-done.8), kind=kOutput, calls=%fused_computation.38 | convolution fusion | flops 4301258752 | bytes 14680064 | tf_op jit(solution)/shard_map/dot_general | solution.py:90
  108.5 3.4 %collective-permute-start = (bf16[30,512]{1,0:T(8,128)(2,1)S(1)}, bf16[30,512]{1,0:T(8,128)(2,1)S(1)}, u32[]{:S(2)}, u32[]{:S(2)}) collective-permute-start(bf16[30,512]{1,0:T(8,128)(2,1)S(1)} %slice.260), channel_id=1, source_target_pairs={{0,4},{4,8},{8,12},{12,16},{16,20},{20,24},{24,28},{1,5},{5,9},{9,... | collective-permute-start | bytes 92168 | tf_op jit(solution)/shard_map/ppermute | solution.py:15
  112.0 1.5 collective-permute-done
  113.5 4.8 %fusion.51 = (f32[512]{0:T(512)S(1)}, f32[512]{0:T(512)S(1)}, f32[512,512]{1,0:T(8,128)S(1)}) fusion(bf16[512,512]{1,0:T(8,128)(2,1)S(1)} %multiply_convert_fusion.2, f32[512]{0:T(512)S(1)} %bitcast.109, bf16[30,512]{1,0:T(8,128)(2,1)S(1)} %collective-permute-done, f32[512]{0:T(512)S(1)} %bitcast.110, f32[512]{0:T(512)S(1)} %bitcast.81, ...), kind=kLoop, calls=%fused_computation.113 | loop fusion | flops 48495616 | bytes 1671168 | tf_op jit(solution)/shard_map/reduce_sum | solution.py:49
  118.4 6.5 %all-reduce = (f32[512]{0:T(512)S(1)}, f32[512]{0:T(512)S(1)}) all-reduce(f32[512]{0:T(512)S(1)} %get-tuple-element.3, f32[512]{0:T(512)S(1)} %get-tuple-element.2), channel_id=1, replica_groups=mesh['ep'=8,'tp'=4] {'tp'}, use_global_device_ids=true, to_apply=%region_3.0 | all-reduce | flops 1024 | bytes 8192 | tf_op jit(solution)/shard_map/psum | solution.py:48
  126.1 40.6 %all-gather.9.cloned.1.call-done = bf16[4096,1024]{1,0:T(8,128)(2,1)} async-done(((bf16[1024,1024]{1,0:T(8,128)(2,1)}), bf16[4096,1024]{1,0:T(8,128)(2,1)}) %all-gather.9.cloned.1.call-update) | async-done | bytes 8388624 | tf_op jit(solution)/shard_map/all_gather | solution.py:8
  166.7 11.5 %copy.22 = bf16[4,1024,1024]{1,2,0:T(8,128)(2,1)} copy(bf16[4,1024,1024]{2,1,0:T(8,128)(2,1)} %bitcast.76) | data formatting | bytes 16777216 | tf_op jit(solution)/shard_map/all_gather | solution.py:8
  178.2 10.1 %fusion.11 = bf16[1024,512]{1,0:T(8,128)(2,1)} fusion(bf16[1024,4096]{0,1:T(8,128)(2,1)} %bitcast.77, bf16[1,4096,512]{2,1,0:T(8,128)(2,1)} %param.28), kind=kOutput, calls=%fused_computation.42 | convolution fusion | flops 4295491584 | bytes 13631488 | tf_op jit(solution)/shard_map/dot_general | solution.py:99
  188.3 5.5 %all-to-all-start.1 = ((bf16[8,128,512]{2,1,0:T(8,128)(2,1)}), bf16[8,128,512]{2,1,0:T(8,128)(2,1)S(1)}, u32[]{:S(2)}, u32[]{:S(2)}) async-start(bf16[8,128,512]{2,1,0:T(8,128)(2,1)} %bitcast.79), calls=%async_computation.1 | async-start | bytes 2097152 | tf_op jit(solution)/shard_map/all_to_all | solution.py:108
  193.9 1.5 fusion.54
  195.4 1.5 fusion.15
  196.9 5.7 %all_gather.19 = bf16[128,512]{1,0:T(8,128)(2,1)S(1)} all-gather(bf16[128,128]{1,0:T(8,128)(2,1)S(1)} %fusion.15), channel_id=1, replica_groups=mesh['ep'=8,'tp'=4] {'tp'}, dimensions={1}, use_global_device_ids=true | all-gather | bytes 163840 | tf_op jit(solution)/shard_map/all_gather | solution.py:103
  202.6 3.6 %convolution_convert_fusion = bf16[512,512]{1,0:T(8,128)(2,1)} fusion(bf16[512,2048]{1,0:T(8,128)(2,1)} %all-gather.5.cloned.1.call-done, bf16[2048,512]{1,0:T(8,128)(2,1)S(1)} %copy-done), kind=kOutput, calls=%fused_computation.45 | convolution fusion | flops 1074003968 | bytes 4718592 | tf_op jit(solution)/shard_map/dot_general | solution.py:58
  206.2 13.8 %all-to-all-done.1 = bf16[8,128,512]{2,1,0:T(8,128)(2,1)S(1)} async-done(((bf16[8,128,512]{2,1,0:T(8,128)(2,1)}), bf16[8,128,512]{2,1,0:T(8,128)(2,1)S(1)}, u32[]{:S(2)}, u32[]{:S(2)}) %all-to-all-start.1) | async-done | bytes 1048608 | tf_op jit(solution)/shard_map/all_to_all | solution.py:108
  220.0 2.6 %gather_fusion = bf16[512,512]{1,0:T(8,128)(2,1)} fusion(bf16[1024,512]{1,0:T(8,128)(2,1)S(1)} %bitcast.75, s32[1024]{0:T(1024)S(1)} %pad_clamp_fusion), kind=kCustom, calls=%fused_computation.1 | custom fusion | bytes 1050624 | tf_op jit(solution)/shard_map/gather | solution.py:111
  222.6 1.4 reshape.141
  224.7 1.9 fusion.14
  (52 shorter events, 6.2 us)
Async XLA Ops:
  7.2 195.4 %copy-start = (bf16[2048,512]{1,0:T(8,128)(2,1)S(1)}, bf16[2048,512]{1,0:T(8,128)(2,1)}, u32[]{:S(2)}) copy-start(bf16[2048,512]{1,0:T(8,128)(2,1)} %param.21) | copy-start | bytes 6291460
  7.2 86.9 %all-gather.7.cloned.1.call-start = ((), (), s32[]{:S(2)}) async-start(), calls=%async_computation.3 | async-start | bytes 5242880 | tf_op jit(solution)/shard_map/all_gather | solution.py:88
  13.3 47.1 %copy-start.1 = (bf16[128,2048]{1,0:T(8,128)(2,1)}, bf16[128,2048]{1,0:T(8,128)(2,1)S(1)}, u32[]{:S(2)}) copy-start(bf16[128,2048]{1,0:T(8,128)(2,1)S(1)} %fusion.18) | copy-start | bytes 1572868
  60.4 106.3 %all-gather.9.cloned.1.call-start = ((), (), s32[]{:S(2)}) async-start(), calls=%async_computation.4 | async-start | bytes 10485760 | tf_op jit(solution)/shard_map/all_gather | solution.py:8
  94.0 7.7 %copy-start.8 = (bf16[1,2048,1024]{2,1,0:T(8,128)(2,1)S(1)}, bf16[1,2048,1024]{2,1,0:T(8,128)(2,1)}, u32[]{:S(2)}) copy-start(bf16[1,2048,1024]{2,1,0:T(8,128)(2,1)} %param.26) | copy-start | bytes 12582916
  94.0 7.7 %copy-start.9 = (bf16[8,128,2048]{2,1,0:T(8,128)(2,1)S(1)}, bf16[8,128,2048]{2,1,0:T(8,128)(2,1)}, u32[]{:S(2)}) copy-start(bf16[8,128,2048]{2,1,0:T(8,128)(2,1)} %all-gather.7.cloned.1.call-done) | copy-start | bytes 12582916
  101.7 6.5 %copy-start.2 = (bf16[512,512]{1,0:T(8,128)(2,1)S(1)}, bf16[512,512]{1,0:T(8,128)(2,1)}, u32[]{:S(2)}) copy-start(bf16[512,512]{1,0:T(8,128)(2,1)} %param.17) | copy-start | bytes 1572868
  101.7 6.5 %copy-start.3 = (bf16[512,512]{1,0:T(8,128)(2,1)S(1)}, bf16[512,512]{1,0:T(8,128)(2,1)}, u32[]{:S(2)}) copy-start(bf16[512,512]{1,0:T(8,128)(2,1)} %param.16) | copy-start | bytes 1572868
  101.7 10.2 %copy-start.4 = (f32[31,512]{1,0:T(8,128)S(1)}, f32[31,512]{1,0:T(8,128)}, u32[]{:S(2)}) copy-start(f32[31,512]{1,0:T(8,128)} %param.18) | copy-start | bytes 190468
  108.1 16.7 %copy-start.5 = (f32[512]{0:T(512)S(1)}, f32[512]{0:T(512)}, u32[]{:S(2)}) copy-start(f32[512]{0:T(512)} %param.20) | copy-start | bytes 6148
  108.1 16.7 %copy-start.6 = (f32[512]{0:T(512)S(1)}, f32[512]{0:T(512)}, u32[]{:S(2)}) copy-start(f32[512]{0:T(512)} %param.19) | copy-start | bytes 6148
  108.2 94.4 %all-gather.5.cloned.1.call-start = ((), (), s32[]{:S(2)}) async-start(), calls=%async_computation.2 | async-start | bytes 2621440 | tf_op jit(solution)/shard_map/all_gather | solution.py:59
  108.5 5.0 %collective-permute-start = (bf16[30,512]{1,0:T(8,128)(2,1)S(1)}, bf16[30,512]{1,0:T(8,128)(2,1)S(1)}, u32[]{:S(2)}, u32[]{:S(2)}) collective-permute-start(bf16[30,512]{1,0:T(8,128)(2,1)S(1)} %slice.260), channel_id=1, source_target_pairs={{0,4},{4,8},{8,12},{12,16},{16,20},{20,24},{24,28},{1,5},{5,9},{9,... | collective-permute-start | bytes 92168 | tf_op jit(solution)/shard_map/ppermute | solution.py:15
  178.2 15.6 %copy-start.7 = (f32[128,4]{0,1:T(4,128)S(1)}, f32[128,4]{0,1:T(4,128)}, u32[]{:S(2)}) copy-start(f32[128,4]{0,1:T(4,128)} %param.25) | copy-start | bytes 6148
  188.3 31.7 %all-to-all-start.1 = ((bf16[8,128,512]{2,1,0:T(8,128)(2,1)}), bf16[8,128,512]{2,1,0:T(8,128)(2,1)S(1)}, u32[]{:S(2)}, u32[]{:S(2)}) async-start(bf16[8,128,512]{2,1,0:T(8,128)(2,1)} %bitcast.79), calls=%async_computation.1 | async-start | bytes 2097152 | tf_op jit(solution)/shard_map/all_to_all | solution.py:108
Sparse Core Ops, SparseCore 0:
  60.5 33.4 all-gather.6
  108.3 58.3 all-gather.8
  168.9 22.5 all-gather.4
